TPU v7x, 32 devices: a whole 2x2x4 slice. The times are simulated.
32 devices in a mesh: sp: 4 (over z), fs: 4 (over y, x), tp: 2 (over core).
Axes of the slice: x: 2, y: 2, z: 4, core: 2. Of those that a mesh axis runs over, the one named last changes fastest.
Arguments:
- tokens: bfloat16 [1024, 2048], P('sp', ('fs', 'tp')), may hold values from -500 to 500
- norm_gain: float32 [2048], replicated, may hold values from 0.1 to 1.9
- query_w: bfloat16 [2048, 1024], P('sp', ('fs', 'tp')), may hold values from -1 to 1
- key_w: bfloat16 [2048, 512], P('sp', ('fs', 'tp')), may hold values from -1 to 1
- value_w: bfloat16 [2048, 512], P('sp', ('fs', 'tp')), may hold values from -0.125 to 0.125
- recept_w: bfloat16 [2048, 1024], P('sp', ('fs', 'tp')), may hold values from -0.125 to 0.125
- rec_key_w: bfloat16 [2048, 1024], P('sp', ('fs', 'tp')), may hold values from -0.125 to 0.125
- rec_value_w: bfloat16 [2048, 1024], P('sp', ('fs', 'tp')), may hold values from -0.125 to 0.125
- decay_down: bfloat16 [2048, 64], replicated, may hold values from -0.125 to 0.125
- decay_up: bfloat16 [64, 1024], replicated, may hold values from -1 to 1
- decay_base: float32 [16, 1024], P(('fs', 'tp'), 'sp'), may hold values from -14 to 0
- learn_rate: float32 [1024], P(('fs', 'tp')), may hold values from 0.1 to 1
- query_gain: float32 [64], replicated, may hold values from 0 to 7
- key_gain: float32 [64], replicated, may hold values from 0 to 7
- sink_logit: float32 [16], P(('fs', 'tp')), may hold values from 1 to 5
- group_gain: float32 [1024], P(('fs', 'tp')), may hold values from 0.1 to 1.9
- out_att_w: bfloat16 [1024, 2048], P(('fs', 'tp'), 'sp'), may hold values from -0.75 to 0.75
- out_rec_w: bfloat16 [1024, 2048], P(('fs', 'tp'), 'sp'), may hold values from -0.1875 to 0.1875
Outputs:
- mixed: bfloat16 [1024, 2048], P(('sp', 'fs', 'tp'))
- row_lse: float32 [16, 1024], P(('fs', 'tp'), 'sp')
All inputs are finite; a program needn't handle non-finite values.
Results may differ from a plain program's by a relative error of at most 0.015.
Values may be sent and summed in bfloat16 or wider, within the bound.
A program may use at most 64 MiB of HBM per device.

v0:
```python
import math
import jax
import jax.numpy as jnp
from jax import lax
from jax.sharding import PartitionSpec as P

HEAD = 64
WINDOW = 128
BLOCK = 32
NORM_EPS = 1e-06
KEY_EPS = 1e-06
GROUP_EPS = 0.00064
EXACT_PRECISION = lax.Precision.HIGHEST


def passed_along(array, axis, by):
    devices = lax.axis_size(axis)
    pairs = [(i, i + by) for i in range(devices) if 0 <= i + by < devices]
    return lax.ppermute(array, axis, pairs)


def prefix(array, axis, combine, identity):
    devices, place = (lax.axis_size(axis), lax.axis_index(axis))
    everything = lax.all_gather(array.astype(jnp.bfloat16), axis)
    start = jnp.broadcast_to(jnp.asarray(identity, array.dtype), array.shape)

    def turn(k, before):
        reached = k < place
        new = combine(before, everything[k].astype(array.dtype))
        return jnp.where(reached, new, before)

    return lax.fori_loop(0, devices, turn, start)


def head_rms(values, gain_vec, num_heads):
    shaped = values.astype(jnp.float32).reshape(values.shape[0], num_heads, HEAD)
    mean_sq = jnp.mean(shaped * shaped, axis=-1, keepdims=True)
    return (shaped * lax.rsqrt(mean_sq + NORM_EPS) * gain_vec).astype(jnp.bfloat16)


def attend(query_rows, key_rows, value_rows, query_gain, key_gain, sink_logit):
    num_rows = query_rows.shape[0]
    num_heads = query_rows.shape[1] // HEAD
    kv_heads = key_rows.shape[1] // HEAD
    group_size = num_heads // kv_heads
    blocks = num_rows // WINDOW
    query_n = head_rms(query_rows, query_gain, num_heads).reshape(
        blocks, WINDOW, kv_heads, group_size, HEAD
    )
    key_n = head_rms(key_rows, key_gain, kv_heads).reshape(num_rows, kv_heads * HEAD)
    paired = jnp.concatenate([key_n, value_rows], axis=1)
    before = passed_along(paired[num_rows - WINDOW :], "sp", 1)
    current = paired.reshape(blocks, WINDOW, 2 * kv_heads * HEAD)
    previous = jnp.concatenate([before[None], current[:-1]], axis=0)
    key_band = jnp.concatenate([previous, current], axis=1).reshape(
        blocks, 2 * WINDOW, 2, kv_heads, HEAD
    )
    scores = jnp.einsum(
        "nqkgd,nskd->nkgqs", query_n, key_band[:, :, 0], preferred_element_type=jnp.float32
    ) * (1.0 / math.sqrt(HEAD))
    offset = lax.axis_index("sp") * num_rows
    lag_table = (
        lax.broadcasted_iota(jnp.int32, (WINDOW, 2 * WINDOW), 0)
        + WINDOW
        - lax.broadcasted_iota(jnp.int32, (WINDOW, 2 * WINDOW), 1)
    )
    key_place = (
        offset
        + (lax.broadcasted_iota(jnp.int32, (blocks, 2 * WINDOW), 0) - 1) * WINDOW
        + lax.broadcasted_iota(jnp.int32, (blocks, 2 * WINDOW), 1)
    )
    allowed = ((lag_table >= 0) & (lag_table < WINDOW))[None, :, :] & (key_place >= 0)[:, None, :]
    allowed = allowed[:, None, None]
    sink_cols = sink_logit.reshape(kv_heads, group_size)[None, :, :, None, None]
    masked = jnp.where(allowed, scores, -jnp.inf)
    row_top = jnp.maximum(jnp.max(masked, axis=-1, keepdims=True), sink_cols)
    weight = jnp.where(allowed, jnp.exp(masked - row_top), 0.0)
    row_total = jnp.sum(weight, axis=-1, keepdims=True) + jnp.exp(sink_cols - row_top)
    row_lse = (
        (row_top + jnp.log(row_total))[..., 0].transpose(1, 2, 0, 3).reshape(num_heads, num_rows)
    )
    att_probs = (weight / row_total).astype(jnp.bfloat16)
    mixed_heads = jnp.einsum(
        "nkgqs,nskd->nqkgd", att_probs, key_band[:, :, 1], preferred_element_type=jnp.float32
    )
    return (mixed_heads.reshape(num_rows, num_heads * HEAD).astype(jnp.bfloat16), row_lse)


def unit_inverse(lower_mat):
    mat_size = lower_mat.shape[-1]
    result = jnp.eye(mat_size, dtype=jnp.float32) + lower_mat
    power_mat = lower_mat
    for section_index in range(mat_size.bit_length() - 2):
        power_mat = jnp.einsum("hij,hjk->hik", power_mat, power_mat, precision=EXACT_PRECISION)
        result = result + jnp.einsum("hij,hjk->hik", result, power_mat, precision=EXACT_PRECISION)
    return result


def pair_table(left_vals, right_vals, allowed):
    return jnp.where(
        allowed, jnp.einsum("hid,hjd->hij", left_vals, right_vals, precision=EXACT_PRECISION), 0.0
    )


def recur(reads, rec_keys, rec_values, log_decay, learn_rate, group_gain):
    num_rows = reads.shape[0]
    num_heads = reads.shape[1] // HEAD
    blocks = num_rows // BLOCK

    def by_block(values):
        return (
            values.astype(jnp.float32).reshape(blocks, BLOCK, num_heads, HEAD).transpose(0, 2, 1, 3)
        )

    read_vals = by_block(reads)
    key_vals = by_block(rec_keys)
    value_vals = by_block(rec_values)
    decay_vals = by_block(log_decay)
    unit_key = key_vals * lax.rsqrt(jnp.sum(key_vals * key_vals, axis=-1, keepdims=True) + KEY_EPS)
    removal = -unit_key
    writing = unit_key * learn_rate.reshape(num_heads, HEAD)[None, :, None, :]
    stacked = jnp.concatenate([jnp.zeros_like(value_vals), value_vals], axis=-1)
    unit_matrix = jnp.broadcast_to(jnp.eye(HEAD, dtype=jnp.float32), (num_heads, HEAD, HEAD))
    start_pair = jnp.concatenate(
        [unit_matrix, jnp.zeros((num_heads, HEAD, HEAD), jnp.float32)], axis=1
    )
    row_iota = lax.broadcasted_iota(jnp.int32, (BLOCK, BLOCK), 0)
    col_iota = lax.broadcasted_iota(jnp.int32, (BLOCK, BLOCK), 1)
    strict = (row_iota > col_iota)[None]
    inclusive = (row_iota >= col_iota)[None]

    def block_step(state_per_block, inputs):
        read_now, key_now, removal_now, writing_now, decay_now, current_value = inputs
        cum_decay = jnp.cumsum(decay_now, axis=1)
        decay_matrix_a = removal_now * jnp.exp(cum_decay - decay_now)
        decay_matrix_b = writing_now * jnp.exp(-cum_decay)
        stacked_key_matrix = key_now * jnp.exp(-cum_decay)
        stacked_receptance = read_now * jnp.exp(cum_decay)
        m_ab = pair_table(decay_matrix_a, decay_matrix_b, strict)
        m_ak = pair_table(decay_matrix_a, stacked_key_matrix, strict)
        m_rb = pair_table(stacked_receptance, decay_matrix_b, inclusive)
        m_rk = pair_table(stacked_receptance, stacked_key_matrix, inclusive)
        right_operand = jnp.einsum(
            "bvq,bzq->bvz", decay_matrix_a, state_per_block, precision=EXACT_PRECISION
        ) + jnp.einsum("hij,hjm->him", m_ak, current_value, precision=EXACT_PRECISION)
        delta_updates = jnp.einsum(
            "hij,hjm->him", unit_inverse(m_ab), right_operand, precision=EXACT_PRECISION
        )
        block_out = (
            jnp.einsum(
                "bvq,bzq->bvz", stacked_receptance, state_per_block, precision=EXACT_PRECISION
            )
            + jnp.einsum("hij,hjm->him", m_rb, delta_updates, precision=EXACT_PRECISION)
            + jnp.einsum("hij,hjm->him", m_rk, current_value, precision=EXACT_PRECISION)
        )
        grown_state = (
            state_per_block
            + jnp.einsum("sao,sac->soc", delta_updates, decay_matrix_b, precision=EXACT_PRECISION)
            + jnp.einsum(
                "sao,sac->soc", current_value, stacked_key_matrix, precision=EXACT_PRECISION
            )
        )
        return (grown_state * jnp.exp(cum_decay[:, -1])[:, None, :], block_out)

    final_state, block_outs = lax.scan(
        block_step, start_pair, (read_vals, key_vals, removal, writing, decay_vals, stacked)
    )

    def chain(earlier, later_pair):
        moved_state = jnp.einsum(
            "hmk,hkj->hmj", earlier, later_pair[:, :HEAD], precision=EXACT_PRECISION
        )
        return moved_state + jnp.concatenate(
            [jnp.zeros_like(later_pair[:, HEAD:]), later_pair[:, HEAD:]], axis=1
        )

    carried = prefix(final_state, "sp", chain, start_pair)
    incoming = carried[:, HEAD:]
    result = block_outs[..., HEAD:] + jnp.einsum(
        "nhlm,hvm->nhlv", block_outs[..., :HEAD], incoming, precision=EXACT_PRECISION
    )
    mean_val = jnp.mean(result, axis=-1, keepdims=True)
    centered = result - mean_val
    variance = jnp.mean(centered * centered, axis=-1, keepdims=True)
    normed = (
        (centered * lax.rsqrt(variance + GROUP_EPS))
        .transpose(0, 2, 1, 3)
        .reshape(num_rows, num_heads * HEAD)
    )
    return (normed * group_gain).astype(jnp.bfloat16)


def per_device(
    tokens,
    norm_gain,
    query_w,
    key_w,
    value_w,
    recept_w,
    rec_key_w,
    rec_value_w,
    decay_down,
    decay_up,
    decay_base,
    learn_rate,
    query_gain,
    key_gain,
    sink_logit,
    group_gain,
    out_att_w,
    out_rec_w,
):
    groups = lax.axis_size(("fs", "tp"))
    own_width = tokens.shape[1]
    own_values = tokens.astype(jnp.float32)
    squares = lax.psum(jnp.sum(own_values * own_values, axis=1), ("fs", "tp"))
    gain_part = lax.dynamic_slice_in_dim(
        norm_gain, lax.axis_index(("fs", "tp")) * own_width, own_width, 0
    )
    scaled = own_values * lax.rsqrt(squares / (own_width * groups) + NORM_EPS)[:, None] * gain_part
    outgoing = scaled.astype(jnp.bfloat16)
    gathered = lax.all_gather(outgoing, ("fs", "tp"), axis=1, tiled=True)

    def rounded(sums):
        return lax.optimization_barrier(
            tuple((acc_total.astype(jnp.bfloat16) for acc_total in sums))
        )

    rec_span = recept_w.shape[1]
    decay_cols = lax.dynamic_slice_in_dim(
        decay_up, lax.axis_index(("fs", "tp")) * rec_span, rec_span, 1
    )
    decay_low = jnp.tanh(jnp.dot(gathered, decay_down, preferred_element_type=jnp.float32)).astype(
        jnp.bfloat16
    )
    decay_rate = jnp.dot(decay_low, decay_cols, preferred_element_type=jnp.float32) + jnp.repeat(
        decay_base.T, HEAD, axis=1
    )
    log_decay = -jnp.exp(decay_rate)
    pieces = (
        lax.all_gather(query_w, "sp", axis=0, tiled=True),
        lax.all_gather(key_w, "sp", axis=0, tiled=True),
        lax.all_gather(value_w, "sp", axis=0, tiled=True),
        lax.all_gather(recept_w, "sp", axis=0, tiled=True),
        lax.all_gather(rec_key_w, "sp", axis=0, tiled=True),
        lax.all_gather(rec_value_w, "sp", axis=0, tiled=True),
    )
    all_sums = tuple(
        (
            jnp.dot(gathered, weight_piece, preferred_element_type=jnp.float32)
            for weight_piece in pieces
        )
    )
    att_inputs = rounded(all_sums[:3])
    att_mix, row_lse = attend(
        att_inputs[0], att_inputs[1], att_inputs[2], query_gain, key_gain, sink_logit
    )
    rec_sums = all_sums[3:]
    rec_inputs = rounded(rec_sums)
    rec_mix = recur(rec_inputs[0], rec_inputs[1], rec_inputs[2], log_decay, learn_rate, group_gain)
    att_full, rec_full = (
        lax.all_gather(out_att_w, "sp", axis=1, tiled=True),
        lax.all_gather(out_rec_w, "sp", axis=1, tiled=True),
    )
    mixed_out = lax.psum_scatter(
        (
            jnp.dot(att_mix, att_full, preferred_element_type=jnp.float32)
            + jnp.dot(rec_mix, rec_full, preferred_element_type=jnp.float32)
        ).astype(jnp.bfloat16),
        ("fs", "tp"),
        scatter_dimension=0,
        tiled=True,
    )
    return (mixed_out, row_lse)


def solution(mesh):
    in_specs = (
        P("sp", ("fs", "tp")),
        P(),
        P("sp", ("fs", "tp")),
        P("sp", ("fs", "tp")),
        P("sp", ("fs", "tp")),
        P("sp", ("fs", "tp")),
        P("sp", ("fs", "tp")),
        P("sp", ("fs", "tp")),
        P(),
        P(),
        P(("fs", "tp"), "sp"),
        P(("fs", "tp")),
        P(),
        P(),
        P(("fs", "tp")),
        P(("fs", "tp")),
        P(("fs", "tp"), "sp"),
        P(("fs", "tp"), "sp"),
    )
    out_specs = (P(("sp", "fs", "tp"), None), P(("fs", "tp"), "sp"))
    return jax.shard_map(
        per_device, mesh=mesh, in_specs=in_specs, out_specs=out_specs, check_vma=False
    )
```

profile of v0, /device:TPU:0, one launch (start us, length us, event | category | flops | bytes accessed | tf_op | source)
XLA Modules:
  0.0 263.2 jit_solution(7685932151415955385)
XLA Ops:
  7.3 1.1 fusion.33
  8.4 15.2 %psum.7 = f32[256]{0:T(256)S(1)} all-reduce(f32[256]{0:T(256)S(1)} %fusion.33), channel_id=1, replica_groups=mesh['sp'=4,'fs'=4,'tp'=2] {'fs','tp'}, use_global_device_ids=true, to_apply=%region_1.0 | all-reduce | flops 256 | bytes 2048 | tf_op jit(solution)/shard_map/psum | solution.py:216
  23.6 0.8 dynamic_slice.33
  24.3 1.7 fusion.35
  26.1 0.7 mul.191
  26.9 0.7 broadcast_in_dim.98
  27.6 0.8 copy.65
  28.4 16.6 %all_gather.35 = bf16[2048,64]{0,1:T(8,128)(2,1)} all-gather(bf16[512,64]{0,1:T(8,128)(2,1)} %param.25), channel_id=1, replica_groups=mesh['sp'=4,'fs'=4,'tp'=2] {'sp'}, dimensions={0}, use_global_device_ids=true | all-gather | bytes 327680 | tf_op jit(solution)/shard_map/all_gather | solution.py:242
  45.0 15.2 %all_gather.36 = bf16[2048,64]{0,1:T(8,128)(2,1)} all-gather(bf16[512,64]{0,1:T(8,128)(2,1)} %param.26), channel_id=1, replica_groups=mesh['sp'=4,'fs'=4,'tp'=2] {'sp'}, dimensions={0}, use_global_device_ids=true | all-gather | bytes 327680 | tf_op jit(solution)/shard_map/all_gather | solution.py:243
  60.2 15.3 %all_gather.34 = bf16[2048,128]{1,0:T(8,128)(2,1)S(1)} all-gather(bf16[512,128]{1,0:T(8,128)(2,1)S(1)} %copy-done.10), channel_id=1, replica_groups=mesh['sp'=4,'fs'=4,'tp'=2] {'sp'}, dimensions={0}, use_global_device_ids=true | all-gather | bytes 655360 | tf_op jit(solution)/shard_map/all_gather | solution.py:241
  75.5 15.5 %all_gather.38 = bf16[2048,128]{1,0:T(8,128)(2,1)S(1)} all-gather(bf16[512,128]{1,0:T(8,128)(2,1)S(1)} %copy-done.11), channel_id=1, replica_groups=mesh['sp'=4,'fs'=4,'tp'=2] {'sp'}, dimensions={0}, use_global_device_ids=true | all-gather | bytes 655360 | tf_op jit(solution)/shard_map/all_gather | solution.py:244
  91.0 16.3 %all_gather.39 = bf16[2048,128]{1,0:T(8,128)(2,1)S(1)} all-gather(bf16[512,128]{1,0:T(8,128)(2,1)S(1)} %copy-done.12), channel_id=1, replica_groups=mesh['sp'=4,'fs'=4,'tp'=2] {'sp'}, dimensions={0}, use_global_device_ids=true | all-gather | bytes 655360 | tf_op jit(solution)/shard_map/all_gather | solution.py:245
  107.3 15.9 %all_gather.40 = bf16[2048,128]{1,0:T(8,128)(2,1)S(1)} all-gather(bf16[512,128]{1,0:T(8,128)(2,1)S(1)} %copy-done.13), channel_id=1, replica_groups=mesh['sp'=4,'fs'=4,'tp'=2] {'sp'}, dimensions={0}, use_global_device_ids=true | all-gather | bytes 655360 | tf_op jit(solution)/shard_map/all_gather | solution.py:246
  123.2 16.1 %all_gather.37 = bf16[128,2048]{1,0:T(8,128)(2,1)} all-gather(bf16[128,512]{1,0:T(8,128)(2,1)S(1)} %copy-done.14), channel_id=1, replica_groups=mesh['sp'=4,'fs'=4,'tp'=2] {'sp'}, dimensions={1}, use_global_device_ids=true | all-gather | bytes 655360 | tf_op jit(solution)/shard_map/all_gather | solution.py:262
  139.3 15.6 %all_gather.43 = bf16[128,2048]{1,0:T(8,128)(2,1)} all-gather(bf16[128,512]{1,0:T(8,128)(2,1)S(1)} %copy-done.15), channel_id=1, replica_groups=mesh['sp'=4,'fs'=4,'tp'=2] {'sp'}, dimensions={1}, use_global_device_ids=true | all-gather | bytes 655360 | tf_op jit(solution)/shard_map/all_gather | solution.py:263
  155.1 0.8 broadcast_and_fusion
  155.8 1.8 convolution_convert_fusion.6
  157.6 1.7 convolution_convert_fusion.5
  159.3 0.4 convolution_convert_fusion.3
  159.9 0.4 convolution_convert_fusion.2
  160.3 0.4 convolution_convert_fusion.1
  160.8 0.4 convolution_convert_fusion
  161.6 1.4 fusion.29
  163.3 3.1 %collective-permute-start = (bf16[128,128]{0,1:T(8,128)(2,1)S(1)}, bf16[128,128]{0,1:T(8,128)(2,1)S(1)}, u32[]{:S(2)}, u32[]{:S(2)}) collective-permute-start(bf16[128,128]{0,1:T(8,128)(2,1)S(1)} %get-tuple-element.242), channel_id=1, source_target_pairs={{0,8},{8,16},{16,24},{1,9},{9,17},{17,25},{2,10},{10,18},{18,26},{... | collective-permute-start | bytes 98312 | tf_op jit(solution)/shard_map/ppermute | solution.py:19
  167.4 35.9 %while.28 = (s32[]{:T(128)}, f32[2,128,64]{1,2,0:T(8,128)S(1)}, f32[8,2,32,128]{3,2,0,1:T(8,128)}, f32[8,2,32,64]{3,2,1,0:T(8,128)S(1)}, f32[8,2,32,64]{3,2,1,0:...) while((s32[]{:T(128)}, f32[2,128,64]{1,2,0:T(8,128)S(1)}, ...), condition=%wide.region_9.10_spmd.clone.clone, body=%wide.region_7.9_spmd.clone.clone.sunk | while | flops 50579456 | bytes 1623177 | solution.py:165
  170.8 0.3 fusion.229
  171.1 0.8 fusion.232
  175.3 0.3 fusion.229
  175.6 0.8 fusion.232
  179.7 0.3 fusion.229
  180.0 0.8 fusion.232
  184.2 0.3 fusion.229
  184.5 0.8 fusion.232
  188.7 0.3 fusion.229
  189.0 0.8 fusion.232
  193.2 0.3 fusion.229
  193.5 0.8 fusion.232
  197.7 0.3 fusion.229
  198.0 0.8 fusion.232
  202.2 0.3 fusion.229
  202.5 0.8 fusion.232
  203.3 13.7 %all-gather = bf16[8,128,64]{1,2,0:T(8,128)(2,1)S(1)} all-gather(bf16[2,128,64]{1,2,0:T(8,128)(2,1)S(1)} %convert_element_type.103), channel_id=2, replica_groups=mesh['sp'=4,'fs'=4,'tp'=2] {'sp'}, dimensions={0}, use_global_device_ids=true | all-gather | bytes 163840 | tf_op jit(solution)/shard_map/all_gather | solution.py:24
  216.9 1.2 while.27
  218.3 0.5 fusion.59
  220.9 0.5 fusion.44
  221.6 1.4 fusion.24
  223.0 0.7 fusion.55
  223.7 32.7 %reduce-scatter.2.cloned.1.call-done = bf16[32,2048]{1,0:T(8,128)(2,1)} async-done(((bf16[256,2048]{1,0:T(8,128)(2,1)}), bf16[32,2048]{1,0:T(8,128)(2,1)}) %reduce-scatter.2.cloned.1.call-update) | async-done | bytes 131088 | tf_op jit(solution)/shard_map/reduce_scatter | solution.py:265
  (310 shorter events, 31.4 us)
Async XLA Ops:
  7.2 154.4 %copy-start = (bf16[2048,64]{0,1:T(8,128)(2,1)S(1)}, bf16[2048,64]{0,1:T(8,128)(2,1)}, u32[]{:S(2)}) copy-start(bf16[2048,64]{0,1:T(8,128)(2,1)} %param.30) | copy-start | bytes 786436
  7.2 53.0 %copy-start.10 = (bf16[512,128]{1,0:T(8,128)(2,1)S(1)}, bf16[512,128]{1,0:T(8,128)(2,1)}, u32[]{:S(2)}) copy-start(bf16[512,128]{1,0:T(8,128)(2,1)} %param.24) | copy-start | bytes 393220
  7.2 68.4 %copy-start.11 = (bf16[512,128]{1,0:T(8,128)(2,1)S(1)}, bf16[512,128]{1,0:T(8,128)(2,1)}, u32[]{:S(2)}) copy-start(bf16[512,128]{1,0:T(8,128)(2,1)} %param.27) | copy-start | bytes 393220
  7.2 83.8 %copy-start.12 = (bf16[512,128]{1,0:T(8,128)(2,1)S(1)}, bf16[512,128]{1,0:T(8,128)(2,1)}, u32[]{:S(2)}) copy-start(bf16[512,128]{1,0:T(8,128)(2,1)} %param.28) | copy-start | bytes 393220
  7.2 100.1 %copy-start.13 = (bf16[512,128]{1,0:T(8,128)(2,1)S(1)}, bf16[512,128]{1,0:T(8,128)(2,1)}, u32[]{:S(2)}) copy-start(bf16[512,128]{1,0:T(8,128)(2,1)} %param.29) | copy-start | bytes 393220
  7.2 148.6 %all-gather.3.cloned.1.call-start = ((), (), s32[]{:S(2)}) async-start(), calls=%async_computation.1 | async-start | bytes 1179648 | tf_op jit(solution)/shard_map/all_gather | solution.py:222
  26.0 97.2 %copy-start.14 = (bf16[128,512]{1,0:T(8,128)(2,1)S(1)}, bf16[128,512]{1,0:T(8,128)(2,1)}, u32[]{:S(2)}) copy-start(bf16[128,512]{1,0:T(8,128)(2,1)} %param.38) | copy-start | bytes 393220
  26.0 230.3 %reduce-scatter.2.cloned.1.call-start = ((), (), s32[]{:S(2)}) async-start(), calls=%async_computation.2 | async-start | bytes 1179648 | tf_op jit(solution)/shard_map/reduce_scatter | solution.py:265
  26.9 112.5 %copy-start.2 = (f32[2,128,64]{1,2,0:T(8,128)}, f32[2,128,64]{1,2,0:T(8,128)S(1)}, u32[]{:S(2)}) copy-start(f32[2,128,64]{1,2,0:T(8,128)S(1)} %concatenate.37) | copy-start | bytes 196612
  27.6 111.7 %copy-start.15 = (bf16[128,512]{1,0:T(8,128)(2,1)S(1)}, bf16[128,512]{1,0:T(8,128)(2,1)}, u32[]{:S(2)}) copy-start(bf16[128,512]{1,0:T(8,128)(2,1)} %param.39) | copy-start | bytes 393220
  155.8 3.5 %copy-start.1 = (bf16[256,2048]{1,0:T(8,128)(2,1)S(1)}, bf16[256,2048]{1,0:T(8,128)(2,1)}, u32[]{:S(2)}) copy-start(bf16[256,2048]{1,0:T(8,128)(2,1)} %all-gather.3.cloned.1.call-done) | copy-start | bytes 3145732
  160.3 1.3 copy-start.7
  160.8 2.5 copy-start.17
  163.0 4.4 %copy-start.4 = (f32[2,128,64]{1,2,0:T(8,128)S(1)}, f32[2,128,64]{1,2,0:T(8,128)}, u32[]{:S(2)}) copy-start(f32[2,128,64]{1,2,0:T(8,128)} %copy-done.2) | copy-start | bytes 196612
  163.3 56.5 %collective-permute-start = (bf16[128,128]{0,1:T(8,128)(2,1)S(1)}, bf16[128,128]{0,1:T(8,128)(2,1)S(1)}, u32[]{:S(2)}, u32[]{:S(2)}) collective-permute-start(bf16[128,128]{0,1:T(8,128)(2,1)S(1)} %get-tuple-element.242), channel_id=1, source_target_pairs={{0,8},{8,16},{16,24},{1,9},{9,17},{17,25},{2,10},{10,18},{18,26},{... | collective-permute-start | bytes 98312 | tf_op jit(solution)/shard_map/ppermute | solution.py:19
  167.4 49.6 %copy-start.3 = (f32[2,128,64]{1,2,0:T(8,128)S(1)}, f32[2,128,64]{1,2,0:T(8,128)}, u32[]{:S(2)}) copy-start(f32[2,128,64]{1,2,0:T(8,128)} %copy-done.2) | copy-start | bytes 196612
  203.2 15.0 %copy-start.8 = (f32[8,2,32,128]{3,2,0,1:T(8,128)S(1)}, f32[8,2,32,128]{3,2,0,1:T(8,128)}, u32[]{:S(2)}) copy-start(f32[8,2,32,128]{3,2,0,1:T(8,128)} %get-tuple-element.157) | copy-start | bytes 786436
  203.3 16.0 %copy-start.18 = (f32[64]{0:T(128)S(1)}, f32[64]{0:T(128)}, u32[]{:S(2)}) copy-start(f32[64]{0:T(128)} %param.34) | copy-start | bytes 772
  218.1 1.8 copy-start.9
  218.2 2.1 copy-start.16
  219.9 1.0 copy-start.6
  220.5 1.1 copy-start.5
  220.5 1.1 copy-start.19
Sparse Core Ops, SparseCore 0:
  26.1 22.8 all-gather.2
  223.1 33.1 reduce-scatter.1
where the time goes:
time: 264 us; the launch traced here: 263 us
  blocking collectives  155 us (59%)
  matrix products  43.7 us (17%)
  waiting for transfers between devices  32.7 us (12%)
  between operations  14.6 us (6%)
  other arithmetic  6.77 us (3%)
  local copies, waits for them, and re-layouts  5.52 us (2%)
  starting transfers between devices  3.16 us (1%)
    reduce_scatter x1, waiting for transfers between devices, per_device(): lax.psum_scatter((jnp.dot(att_mix, att_full, preferred_element_type=jnp.f...  32.7 us
    all_gather x1, blocking collectives, per_device(): lax.all_gather(key_w, 'sp', axis=0, tiled=True)  16.6 us
    all_gather x1, blocking collectives, per_device(): lax.all_gather(rec_key_w, 'sp', axis=0, tiled=True)  16.3 us
    all_gather x1, blocking collectives, per_device(): lax.all_gather(out_att_w, 'sp', axis=1, tiled=True)  16.1 us
    all_gather x1, blocking collectives, per_device(): lax.all_gather(rec_value_w, 'sp', axis=0, tiled=True)  15.9 us
    all_gather x1, blocking collectives, per_device(): lax.all_gather(out_rec_w, 'sp', axis=1, tiled=True)  15.6 us
    all_gather x1, blocking collectives, per_device(): lax.all_gather(recept_w, 'sp', axis=0, tiled=True)  15.5 us
    all_gather x1, blocking collectives, per_device(): lax.all_gather(query_w, 'sp', axis=0, tiled=True)  15.3 us
  transfers between devices with their start and end apart: 3, of which 1 were waited for; matrix products, arithmetic and copies ran while one was open for 16% of the time, Pallas kernels for 0%

commit v1 on v0

--- a/solution.py
+++ b/solution.py
@@ -213,7 +213,8 @@
     groups = lax.axis_size(("fs", "tp"))
     own_width = tokens.shape[1]
     own_values = tokens.astype(jnp.float32)
-    squares = lax.psum(jnp.sum(own_values * own_values, axis=1), ("fs", "tp"))
+    partial = lax.psum(jnp.sum(own_values * own_values, axis=1), "fs")
+    squares = lax.psum(partial, "tp")
     gain_part = lax.dynamic_slice_in_dim(
         norm_gain, lax.axis_index(("fs", "tp")) * own_width, own_width, 0
     )

time: 264 us -> 263 us (level)
    psum x1 -> x2, blocking collectives: 15.2 us -> 13.8 us  [the longest x1 11.4 us: per_device(): partial = lax.psum(jnp.sum(own_values * own_values, axis=1), 'fs')]
where the time goes in v1:
time: 263 us; the launch traced here: 262 us
  blocking collectives  153 us (58%)
  matrix products  43.7 us (17%)
  waiting for transfers between devices  33.9 us (13%)
  between operations  14.6 us (6%)
  other arithmetic  6.78 us (3%)
  local copies, waits for them, and re-layouts  5.51 us (2%)
  starting transfers between devices  3.96 us (2%)
    reduce_scatter x1, waiting for transfers between devices, per_device(): lax.psum_scatter((jnp.dot(att_mix, att_full, preferred_element_type=jnp.f...  33.9 us
    all_gather x1, blocking collectives, per_device(): lax.all_gather(key_w, 'sp', axis=0, tiled=True)  16.2 us
    all_gather x1, blocking collectives, per_device(): lax.all_gather(rec_key_w, 'sp', axis=0, tiled=True)  16.1 us
    all_gather x1, blocking collectives, per_device(): lax.all_gather(out_rec_w, 'sp', axis=1, tiled=True)  15.8 us
    all_gather x1, blocking collectives, per_device(): lax.all_gather(query_w, 'sp', axis=0, tiled=True)  15.7 us
    all_gather x1, blocking collectives, per_device(): lax.all_gather(recept_w, 'sp', axis=0, tiled=True)  15.7 us
    all_gather x1, blocking collectives, per_device(): lax.all_gather(out_att_w, 'sp', axis=1, tiled=True)  15.5 us
    all_gather x1, blocking collectives, per_device(): lax.all_gather(value_w, 'sp', axis=0, tiled=True)  15.4 us
  transfers between devices with their start and end apart: 3, of which 1 were waited for; matrix products, arithmetic and copies ran while one was open for 16% of the time, Pallas kernels for 0%

profile of v1, /device:TPU:0, one launch (start us, length us, event | category | flops | bytes accessed | tf_op | source)
XLA Modules:
  0.0 262.4 jit_solution(3848021720956799064)
XLA Ops:
  7.3 1.1 fusion.33
  8.4 11.4 %psum.14 = f32[256]{0:T(256)S(1)} all-reduce(f32[256]{0:T(256)S(1)} %fusion.33), channel_id=1, replica_groups=mesh['sp'=4,'fs'=4,'tp'=2] {'fs'}, use_global_device_ids=true, to_apply=%region_1.0 | all-reduce | flops 256 | bytes 2048 | tf_op jit(solution)/shard_map/psum | solution.py:216
  19.8 2.5 psum.15
  22.3 0.8 dynamic_slice.33
  23.0 1.7 fusion.35
  24.8 0.7 mul.191
  25.6 0.7 broadcast_in_dim.98
  26.3 0.7 copy.65
  27.1 16.2 %all_gather.35 = bf16[2048,64]{0,1:T(8,128)(2,1)} all-gather(bf16[512,64]{0,1:T(8,128)(2,1)} %param.25), channel_id=1, replica_groups=mesh['sp'=4,'fs'=4,'tp'=2] {'sp'}, dimensions={0}, use_global_device_ids=true | all-gather | bytes 327680 | tf_op jit(solution)/shard_map/all_gather | solution.py:243
  43.3 15.4 %all_gather.36 = bf16[2048,64]{0,1:T(8,128)(2,1)} all-gather(bf16[512,64]{0,1:T(8,128)(2,1)} %param.26), channel_id=1, replica_groups=mesh['sp'=4,'fs'=4,'tp'=2] {'sp'}, dimensions={0}, use_global_device_ids=true | all-gather | bytes 327680 | tf_op jit(solution)/shard_map/all_gather | solution.py:244
  58.7 15.7 %all_gather.34 = bf16[2048,128]{1,0:T(8,128)(2,1)S(1)} all-gather(bf16[512,128]{1,0:T(8,128)(2,1)S(1)} %copy-done.10), channel_id=1, replica_groups=mesh['sp'=4,'fs'=4,'tp'=2] {'sp'}, dimensions={0}, use_global_device_ids=true | all-gather | bytes 655360 | tf_op jit(solution)/shard_map/all_gather | solution.py:242
  74.3 15.7 %all_gather.38 = bf16[2048,128]{1,0:T(8,128)(2,1)S(1)} all-gather(bf16[512,128]{1,0:T(8,128)(2,1)S(1)} %copy-done.11), channel_id=1, replica_groups=mesh['sp'=4,'fs'=4,'tp'=2] {'sp'}, dimensions={0}, use_global_device_ids=true | all-gather | bytes 655360 | tf_op jit(solution)/shard_map/all_gather | solution.py:245
  90.0 16.1 %all_gather.39 = bf16[2048,128]{1,0:T(8,128)(2,1)S(1)} all-gather(bf16[512,128]{1,0:T(8,128)(2,1)S(1)} %copy-done.12), channel_id=1, replica_groups=mesh['sp'=4,'fs'=4,'tp'=2] {'sp'}, dimensions={0}, use_global_device_ids=true | all-gather | bytes 655360 | tf_op jit(solution)/shard_map/all_gather | solution.py:246
  106.1 14.7 %all_gather.40 = bf16[2048,128]{1,0:T(8,128)(2,1)S(1)} all-gather(bf16[512,128]{1,0:T(8,128)(2,1)S(1)} %copy-done.13), channel_id=1, replica_groups=mesh['sp'=4,'fs'=4,'tp'=2] {'sp'}, dimensions={0}, use_global_device_ids=true | all-gather | bytes 655360 | tf_op jit(solution)/shard_map/all_gather | solution.py:247
  120.8 15.5 %all_gather.37 = bf16[128,2048]{1,0:T(8,128)(2,1)} all-gather(bf16[128,512]{1,0:T(8,128)(2,1)S(1)} %copy-done.14), channel_id=1, replica_groups=mesh['sp'=4,'fs'=4,'tp'=2] {'sp'}, dimensions={1}, use_global_device_ids=true | all-gather | bytes 655360 | tf_op jit(solution)/shard_map/all_gather | solution.py:263
  136.3 15.8 %all_gather.43 = bf16[128,2048]{1,0:T(8,128)(2,1)} all-gather(bf16[128,512]{1,0:T(8,128)(2,1)S(1)} %copy-done.15), channel_id=1, replica_groups=mesh['sp'=4,'fs'=4,'tp'=2] {'sp'}, dimensions={1}, use_global_device_ids=true | all-gather | bytes 655360 | tf_op jit(solution)/shard_map/all_gather | solution.py:264
  152.2 0.8 broadcast_and_fusion
  153.0 1.8 convolution_convert_fusion.6
  154.8 1.7 convolution_convert_fusion.5
  156.5 0.4 convolution_convert_fusion.3
  157.1 0.4 convolution_convert_fusion.2
  157.5 0.4 convolution_convert_fusion.1
  157.9 0.4 convolution_convert_fusion
  158.8 1.4 fusion.29
  160.5 3.9 %collective-permute-start = (bf16[128,128]{0,1:T(8,128)(2,1)S(1)}, bf16[128,128]{0,1:T(8,128)(2,1)S(1)}, u32[]{:S(2)}, u32[]{:S(2)}) collective-permute-start(bf16[128,128]{0,1:T(8,128)(2,1)S(1)} %get-tuple-element.242), channel_id=1, source_target_pairs={{0,8},{8,16},{16,24},{1,9},{9,17},{17,25},{2,10},{10,18},{18,26},{... | collective-permute-start | bytes 98312 | tf_op jit(solution)/shard_map/ppermute | solution.py:19
  165.3 35.9 %while.28 = (s32[]{:T(128)}, f32[2,128,64]{1,2,0:T(8,128)S(1)}, f32[8,2,32,128]{3,2,0,1:T(8,128)}, f32[8,2,32,64]{3,2,1,0:T(8,128)S(1)}, f32[8,2,32,64]{3,2,1,0:...) while((s32[]{:T(128)}, f32[2,128,64]{1,2,0:T(8,128)S(1)}, ...), condition=%wide.region_10.11_spmd.clone.clone, body=%wide.region_8.10_spmd.clone.clone.sunk | while | flops 50579456 | bytes 1623177 | solution.py:165
  168.8 0.3 fusion.229
  169.1 0.8 fusion.232
  173.2 0.3 fusion.229
  173.5 0.8 fusion.232
  177.7 0.3 fusion.229
  178.0 0.8 fusion.232
  182.2 0.3 fusion.229
  182.5 0.8 fusion.232
  186.7 0.3 fusion.229
  187.0 0.8 fusion.232
  191.1 0.3 fusion.229
  191.4 0.8 fusion.232
  195.6 0.3 fusion.229
  195.9 0.8 fusion.232
  200.4 0.8 fusion.232
  201.2 13.6 %all-gather = bf16[8,128,64]{1,2,0:T(8,128)(2,1)S(1)} all-gather(bf16[2,128,64]{1,2,0:T(8,128)(2,1)S(1)} %convert_element_type.103), channel_id=2, replica_groups=mesh['sp'=4,'fs'=4,'tp'=2] {'sp'}, dimensions={0}, use_global_device_ids=true | all-gather | bytes 163840 | tf_op jit(solution)/shard_map/all_gather | solution.py:24
  214.9 1.2 while.27
  216.2 0.5 fusion.59
  218.9 0.5 fusion.44
  219.5 1.4 fusion.24
  221.0 0.7 fusion.55
  221.6 33.9 %reduce-scatter.2.cloned.1.call-done = bf16[32,2048]{1,0:T(8,128)(2,1)} async-done(((bf16[256,2048]{1,0:T(8,128)(2,1)}), bf16[32,2048]{1,0:T(8,128)(2,1)}) %reduce-scatter.2.cloned.1.call-update) | async-done | bytes 131088 | tf_op jit(solution)/shard_map/reduce_scatter | solution.py:266
  (311 shorter events, 31.7 us)
Async XLA Ops:
  7.2 151.6 %copy-start = (bf16[2048,64]{0,1:T(8,128)(2,1)S(1)}, bf16[2048,64]{0,1:T(8,128)(2,1)}, u32[]{:S(2)}) copy-start(bf16[2048,64]{0,1:T(8,128)(2,1)} %param.30) | copy-start | bytes 786436
  7.2 51.5 %copy-start.10 = (bf16[512,128]{1,0:T(8,128)(2,1)S(1)}, bf16[512,128]{1,0:T(8,128)(2,1)}, u32[]{:S(2)}) copy-start(bf16[512,128]{1,0:T(8,128)(2,1)} %param.24) | copy-start | bytes 393220
  7.2 67.1 %copy-start.11 = (bf16[512,128]{1,0:T(8,128)(2,1)S(1)}, bf16[512,128]{1,0:T(8,128)(2,1)}, u32[]{:S(2)}) copy-start(bf16[512,128]{1,0:T(8,128)(2,1)} %param.27) | copy-start | bytes 393220
  7.2 82.8 %copy-start.12 = (bf16[512,128]{1,0:T(8,128)(2,1)S(1)}, bf16[512,128]{1,0:T(8,128)(2,1)}, u32[]{:S(2)}) copy-start(bf16[512,128]{1,0:T(8,128)(2,1)} %param.28) | copy-start | bytes 393220
  7.2 98.9 %copy-start.13 = (bf16[512,128]{1,0:T(8,128)(2,1)S(1)}, bf16[512,128]{1,0:T(8,128)(2,1)}, u32[]{:S(2)}) copy-start(bf16[512,128]{1,0:T(8,128)(2,1)} %param.29) | copy-start | bytes 393220
  7.2 145.8 %all-gather.3.cloned.1.call-start = ((), (), s32[]{:S(2)}) async-start(), calls=%async_computation.1 | async-start | bytes 1179648 | tf_op jit(solution)/shard_map/all_gather | solution.py:223
  24.7 96.1 %copy-start.14 = (bf16[128,512]{1,0:T(8,128)(2,1)S(1)}, bf16[128,512]{1,0:T(8,128)(2,1)}, u32[]{:S(2)}) copy-start(bf16[128,512]{1,0:T(8,128)(2,1)} %param.38) | copy-start | bytes 393220
  24.7 230.8 %reduce-scatter.2.cloned.1.call-start = ((), (), s32[]{:S(2)}) async-start(), calls=%async_computation.2 | async-start | bytes 1179648 | tf_op jit(solution)/shard_map/reduce_scatter | solution.py:266
  25.6 110.7 %copy-start.2 = (f32[2,128,64]{1,2,0:T(8,128)}, f32[2,128,64]{1,2,0:T(8,128)S(1)}, u32[]{:S(2)}) copy-start(f32[2,128,64]{1,2,0:T(8,128)S(1)} %concatenate.37) | copy-start | bytes 196612
  26.3 110.0 %copy-start.15 = (bf16[128,512]{1,0:T(8,128)(2,1)S(1)}, bf16[128,512]{1,0:T(8,128)(2,1)}, u32[]{:S(2)}) copy-start(bf16[128,512]{1,0:T(8,128)(2,1)} %param.39) | copy-start | bytes 393220
  153.0 3.5 %copy-start.1 = (bf16[256,2048]{1,0:T(8,128)(2,1)S(1)}, bf16[256,2048]{1,0:T(8,128)(2,1)}, u32[]{:S(2)}) copy-start(bf16[256,2048]{1,0:T(8,128)(2,1)} %all-gather.3.cloned.1.call-done) | copy-start | bytes 3145732
  157.5 1.3 copy-start.7
  157.9 2.5 copy-start.17
  160.2 5.2 %copy-start.4 = (f32[2,128,64]{1,2,0:T(8,128)S(1)}, f32[2,128,64]{1,2,0:T(8,128)}, u32[]{:S(2)}) copy-start(f32[2,128,64]{1,2,0:T(8,128)} %copy-done.2) | copy-start | bytes 196612
  160.5 57.3 %collective-permute-start = (bf16[128,128]{0,1:T(8,128)(2,1)S(1)}, bf16[128,128]{0,1:T(8,128)(2,1)S(1)}, u32[]{:S(2)}, u32[]{:S(2)}) collective-permute-start(bf16[128,128]{0,1:T(8,128)(2,1)S(1)} %get-tuple-element.242), channel_id=1, source_target_pairs={{0,8},{8,16},{16,24},{1,9},{9,17},{17,25},{2,10},{10,18},{18,26},{... | collective-permute-start | bytes 98312 | tf_op jit(solution)/shard_map/ppermute | solution.py:19
  165.3 49.5 %copy-start.3 = (f32[2,128,64]{1,2,0:T(8,128)S(1)}, f32[2,128,64]{1,2,0:T(8,128)}, u32[]{:S(2)}) copy-start(f32[2,128,64]{1,2,0:T(8,128)} %copy-done.2) | copy-start | bytes 196612
  201.2 15.0 %copy-start.8 = (f32[8,2,32,128]{3,2,0,1:T(8,128)S(1)}, f32[8,2,32,128]{3,2,0,1:T(8,128)}, u32[]{:S(2)}) copy-start(f32[8,2,32,128]{3,2,0,1:T(8,128)} %get-tuple-element.157) | copy-start | bytes 786436
  201.2 16.0 %copy-start.18 = (f32[64]{0:T(128)S(1)}, f32[64]{0:T(128)}, u32[]{:S(2)}) copy-start(f32[64]{0:T(128)} %param.34) | copy-start | bytes 772
  216.1 1.8 copy-start.9
  216.1 2.1 copy-start.16
  217.8 1.0 copy-start.6
  218.5 1.1 copy-start.5
  218.5 1.1 copy-start.19
Sparse Core Ops, SparseCore 0:
  24.8 22.8 all-gather.2
  221.1 34.4 reduce-scatter.1
